TPU v7x, 32 devices: a whole 2x2x4 slice. The times are simulated.
32 devices in a mesh: grp: 2 (over y), sp: 4 (over z), tp: 4 (over x, core).
Axes of the slice: x: 2, y: 2, z: 4, core: 2. Of those that a mesh axis runs over, the one named last changes fastest.
Arguments:
- skip_stream: bfloat16 [1024, 2048], P(('grp', 'sp', 'tp')), parts along dimension 0, may hold values from -6 to 6
- wide_probe_logits: bfloat16 [1024, 512], P(('grp', 'sp'), 'tp'), parts along dimension 0, may hold values from -6 to 6
- narrow_probe_logits: bfloat16 [1024, 512], P(('grp', 'sp'), 'tp'), parts along dimension 0, may hold values from -6 to 6
- wide_decay_logits: bfloat16 [1024, 512], P(('grp', 'sp'), 'tp'), parts along dimension 0, may hold values from -7.5 to 7.5
- narrow_decay_logits: bfloat16 [1024, 512], P(('grp', 'sp'), 'tp'), parts along dimension 0, may hold values from -7.5 to 7.5
- wide_floor_complement: float32 [2, 512], P(None, 'tp'), may hold values from 0.0002734375 to 0.21
- narrow_floor_complement: float32 [2, 512], P(None, 'tp'), may hold values from 0.0002734375 to 0.21
- payloads: bfloat16 [1024, 1536], P(('grp', 'sp'), 'tp'), parts along dimension 0, may hold values from -6 to 6
- result_switch_logits: bfloat16 [1024, 1536], P(('grp', 'sp'), 'tp'), parts along dimension 0, may hold values from -6 to 6
- spike_decays: float32 [1024, 12], P(('grp', 'sp'), 'tp'), parts along dimension 0, may hold values from -1.5 to 0
- channel_scale_vector: float32 [1536], P('tp'), may hold values from 0.1 to 1.9
- result_mapping_matrix: bfloat16 [1536, 2048], P('tp'), may hold values from -0.15625 to 0.15625
- specialist_scale_vector: float32 [2048], replicated, may hold values from 0.1 to 1.9
- assignments: int32 [1024, 2], P(('grp', 'sp', 'tp')), parts along dimension 0, may hold values from 0 to 3, all different within a row; in each aligned block of 32 rows (0 to 31, 32 to 63, ...) at most 32 rows name the same one
- assignment_share: float32 [1024, 2], P(('grp', 'sp', 'tp')), parts along dimension 0, may hold values from 0.2 to 1
- specialist_switch_matrix: bfloat16 [4, 2048, 3584], P('sp', None, 'tp'), may hold values from -0.125 to 0.125
- specialist_raising_matrix: bfloat16 [4, 2048, 3584], P('sp', None, 'tp'), may hold values from -0.125 to 0.125
- specialist_lowering_matrix: bfloat16 [4, 3584, 2048], P('sp', 'tp'), may hold values from -0.09375 to 0.09375
Outputs:
- layer_output: bfloat16 [1024, 2048], P(('grp', 'sp', 'tp')), parts along dimension 0
There are 2 independent parts, one for each index of `grp`. A program takes and returns all parts, laid end to end along the dimension named above; an argument that names none is the same for every part. Nothing has to cross between parts.
Inputs may be any that keep to these rules, and one draw needn't show every extreme that they name: `assignments`: each row names 2 different experts; in each aligned block of 32 rows no expert is named by more than 32 rows, a bound that some block reaches.
All inputs are finite; a program needn't handle non-finite values.
Results may differ from a plain program's by a relative error of at most 0.015.
Values may be sent and summed in bfloat16 or wider, within the bound.
A program may use at most 128 MiB of HBM per device.

v0:
```python
import jax
import jax.numpy as jnp
from jax import lax
from jax.sharding import PartitionSpec as P

D = 2048
WIDE_LOOKUP_WIDTH = 128
NARROW_LOOKUP = 64
PAYLOAD_EXTENT = 128
BLOCK = 64


epsilon = 1e-06


def carried_in(value, axis, join, neutral, backward):
    count = lax.axis_size(axis)
    place = lax.axis_index(axis)
    ahead = count - 1 - place if backward else place
    gathered = jax.tree.map(
        lambda a, kind: lax.all_gather(a.astype(kind), axis),
        value,
        jax.tree.map(lambda a: jnp.bfloat16 if a.dtype == jnp.float32 else a.dtype, value),
    )
    state = jax.tree.map(lambda a, e: jnp.zeros_like(a) + jnp.asarray(e, a.dtype), value, neutral)

    def one(lap, state):
        source = count - 1 - lap if backward else lap
        return join(
            state,
            jax.tree.map(
                lambda a, own: lax.dynamic_index_in_dim(a, source, 0, False).astype(own.dtype),
                gathered,
                value,
            ),
        )

    return lax.fori_loop(0, ahead, one, state)


def switch_cumulants(decay_factor, floor_complement, spike_log_decay):
    initial_memory = jax.nn.sigmoid(-decay_factor)
    key_input = floor_complement * initial_memory
    keep_log_decay = jnp.log1p(-floor_complement * initial_memory) + spike_log_decay[:, :, None]
    return (key_input, keep_log_decay)


def block_pass(queries, key_input, memory_matrix, keep_log_decay, initial):
    series_extent = queries.shape[0]
    channel_tally = queries.shape[1]
    block_count = series_extent // BLOCK

    def to_blocks(tensor):
        return tensor.reshape(block_count, BLOCK, channel_tally, tensor.shape[-1]).transpose(
            0, 2, 1, 3
        )

    below_mask = jnp.tril(jnp.ones((BLOCK, BLOCK), dtype=bool))[None, :, :, None]

    def advance(carried, segment):
        query_block, key_block, value_block, decay_block = segment
        running = jnp.cumsum(decay_block, axis=1)
        log_gap = running[:, :, None, :] - running[:, None, :, :]
        weight = jnp.where(below_mask, jnp.exp(jnp.where(below_mask, log_gap, 0.0)), 0.0)
        scores = jnp.einsum(
            "htd,hsd,htsd->hts", query_block, key_block, weight, precision=lax.Precision.HIGHEST
        )
        output = jnp.einsum("hts,hse->hte", scores, value_block, precision=lax.Precision.HIGHEST)
        output = output + jnp.einsum(
            "htd,hde->hte", query_block * jnp.exp(running), carried, precision=lax.Precision.HIGHEST
        )
        closing = running[:, -1:, :]
        fresh = jnp.einsum(
            "hsd,hse->hde",
            key_block * jnp.exp(closing - running),
            value_block,
            precision=lax.Precision.HIGHEST,
        )
        carried = jnp.exp(closing[:, 0, :, None]) * carried + fresh
        return (carried, output)

    closing_state, outputs = lax.scan(
        advance,
        initial,
        (
            to_blocks(queries),
            to_blocks(key_input),
            to_blocks(memory_matrix),
            to_blocks(keep_log_decay),
        ),
    )
    return (outputs.transpose(0, 2, 1, 3).reshape(series_extent, channel_tally, -1), closing_state)


def summary_terms(key_input, memory_matrix, keep_log_decay):
    running = jnp.cumsum(keep_log_decay, axis=0)
    closing = running[-1]
    carried = jnp.einsum(
        "thd,the->hde",
        key_input * jnp.exp(closing[None] - running),
        memory_matrix,
        precision=lax.Precision.HIGHEST,
    )
    return (closing, carried)


def combine_states(earlier, following):
    decay_one, state_one, decay_two, state_two = earlier
    later_one, fresh_one, later_two, fresh_two = following
    return (
        decay_one + later_one,
        jnp.exp(later_one)[:, :, None] * state_one + fresh_one,
        decay_two + later_two,
        jnp.exp(later_two)[:, :, None] * state_two + fresh_two,
    )


def states_before(summaries):
    blank = jax.tree.map(jnp.zeros_like, summaries)
    return carried_in(summaries, "sp", combine_states, blank, False)


def states_after(summaries):
    blank = jax.tree.map(jnp.zeros_like, summaries)
    return carried_in(summaries, "sp", combine_states, blank, True)


def grouped_inputs(
    probe_logits, decay_factor, floor_complement, spike_log_decay, memory_matrix, lookup_extent
):
    series_extent = probe_logits.shape[0]
    channel_tally = spike_log_decay.shape[1]
    queries = jax.nn.silu(
        probe_logits.astype(jnp.float32).reshape(series_extent, channel_tally, lookup_extent)
    ) * lookup_extent ** (-0.5)
    decay_switch_level = decay_factor.astype(jnp.float32).reshape(
        series_extent, channel_tally, lookup_extent
    )
    onward_lookup, onward_log_decay = switch_cumulants(
        decay_switch_level,
        floor_complement[0].reshape(channel_tally, lookup_extent),
        spike_log_decay,
    )
    reverse_lookup, reverse_log_decay = switch_cumulants(
        decay_switch_level,
        floor_complement[1].reshape(channel_tally, lookup_extent),
        spike_log_decay,
    )
    forward = (queries, onward_lookup, memory_matrix, onward_log_decay)
    backward = (
        jnp.flip(queries, axis=0),
        jnp.flip(reverse_lookup, axis=0),
        jnp.flip(memory_matrix, axis=0),
        jnp.flip(reverse_log_decay, axis=0),
    )
    return (forward, backward)


def one_direction(broad_side, slim_side, carry_states):
    broad_decay, broad_end = summary_terms(broad_side[1], broad_side[2], broad_side[3])
    slim_decay, slim_end = summary_terms(slim_side[1], slim_side[2], slim_side[3])
    entering = carry_states((broad_decay, broad_end, slim_decay, slim_end))
    broad_out = block_pass(broad_side[0], broad_side[1], broad_side[2], broad_side[3], entering[1])[
        0
    ]
    slim_out = block_pass(slim_side[0], slim_side[1], slim_side[2], slim_side[3], entering[3])[0]
    return (broad_out, slim_out)


def local(
    skip_stream,
    wide_probe_logits,
    narrow_probe_logits,
    wide_decay_logits,
    narrow_decay_logits,
    wide_floor_complement,
    narrow_floor_complement,
    payloads,
    result_switch_logits,
    spike_decays,
    channel_scale_vector,
    result_mapping_matrix,
    specialist_scale_vector,
    assignments,
    assignment_share,
    specialist_switch_matrix,
    specialist_raising_matrix,
    specialist_lowering_matrix,
):
    series_extent = wide_probe_logits.shape[0]
    clustered_channels = wide_probe_logits.shape[1] // WIDE_LOOKUP_WIDTH
    joint_heads = 3 * clustered_channels
    memory_matrix = payloads.astype(jnp.float32).reshape(
        series_extent, clustered_channels, 3, PAYLOAD_EXTENT
    )
    spike_span = spike_decays.reshape(series_extent, clustered_channels, 3)
    broad_sides = grouped_inputs(
        wide_probe_logits,
        wide_decay_logits,
        wide_floor_complement,
        spike_span[:, :, 0],
        memory_matrix[:, :, 0],
        WIDE_LOOKUP_WIDTH,
    )
    slim_sides = grouped_inputs(
        narrow_probe_logits,
        narrow_decay_logits,
        narrow_floor_complement,
        spike_span[:, :, 1:].reshape(series_extent, 2 * clustered_channels),
        memory_matrix[:, :, 1:].reshape(series_extent, 2 * clustered_channels, PAYLOAD_EXTENT),
        NARROW_LOOKUP,
    )
    ahead_broad, ahead_slim = one_direction(broad_sides[0], slim_sides[0], states_before)
    behind_broad, behind_slim = one_direction(broad_sides[1], slim_sides[1], states_after)
    wide_channel_slices = ahead_broad + jnp.flip(behind_broad, axis=0)
    narrow_channel_slices = ahead_slim + jnp.flip(behind_slim, axis=0)
    joined = jnp.concatenate(
        [
            wide_channel_slices[:, :, None],
            narrow_channel_slices.reshape(series_extent, clustered_channels, 2, PAYLOAD_EXTENT),
        ],
        axis=2,
    ).reshape(series_extent, joint_heads, PAYLOAD_EXTENT)
    normed_heads = joined * lax.rsqrt(jnp.mean(joined * joined, axis=-1, keepdims=True) + epsilon)
    gated_heads = (
        normed_heads
        * channel_scale_vector.reshape(joint_heads, PAYLOAD_EXTENT)
        * jax.nn.silu(
            result_switch_logits.astype(jnp.float32).reshape(
                series_extent, joint_heads, PAYLOAD_EXTENT
            )
        )
    )
    mixed_heads = gated_heads.reshape(series_extent, joint_heads * PAYLOAD_EXTENT).astype(
        jnp.bfloat16
    )
    row_count = skip_stream.shape[0]
    mixing = lax.psum_scatter(
        jnp.dot(mixed_heads, result_mapping_matrix, preferred_element_type=jnp.float32).astype(
            jnp.bfloat16
        ),
        "tp",
        scatter_dimension=0,
        tiled=True,
    ).astype(jnp.float32)
    hidden_float = (
        (skip_stream.astype(jnp.float32) + mixing).astype(jnp.bfloat16).astype(jnp.float32)
    )
    normed = (
        hidden_float
        * lax.rsqrt(jnp.mean(hidden_float * hidden_float, axis=-1, keepdims=True) + epsilon)
        * specialist_scale_vector
    ).astype(jnp.bfloat16)
    expert_count = lax.axis_size("sp")
    shard_count = lax.axis_size("tp")
    top_count = assignments.shape[1]
    capacity = max(2, 2 * row_count * top_count // expert_count)
    slot_total = expert_count * capacity
    flat_routes = assignments.reshape(-1)
    member = (flat_routes[:, None] == jnp.arange(expert_count, dtype=jnp.int32)[None, :]).astype(
        jnp.int32
    )
    earlier_count = jnp.cumsum(member, axis=0) - member
    slot_index = flat_routes * capacity + jnp.sum(earlier_count * member, axis=1)
    picker = (slot_index[:, None] == jnp.arange(slot_total, dtype=jnp.int32)[None, :]).astype(
        jnp.bfloat16
    )
    dispatch = jnp.sum(picker.reshape(row_count, top_count, slot_total), axis=1)
    outgoing = (
        jnp.einsum("rs,rd->sd", dispatch, normed, preferred_element_type=jnp.float32)
        .astype(jnp.bfloat16)
        .reshape(expert_count, capacity, D)
    )
    arrived = lax.all_gather(
        lax.all_to_all(outgoing, "sp", split_axis=0, concat_axis=0, tiled=True),
        "tp",
        axis=0,
        tiled=True,
    )
    flat_rows = arrived.reshape(-1, D)
    gate_part = jnp.dot(flat_rows, specialist_switch_matrix[0], preferred_element_type=jnp.float32)
    up_part = jnp.dot(flat_rows, specialist_raising_matrix[0], preferred_element_type=jnp.float32)
    activated = (
        (jax.nn.silu(gate_part) * up_part)
        .astype(jnp.bfloat16)
        .reshape(arrived.shape[0], arrived.shape[1], -1)
    )
    by_source = activated.reshape(shard_count, expert_count, capacity, -1)
    per_column = expert_count * capacity
    row_block = by_source.reshape(per_column * lax.axis_size("tp"), -1)
    partial_value = jnp.dot(
        row_block, specialist_lowering_matrix[0], preferred_element_type=jnp.float32
    )
    summed = lax.psum_scatter(
        lax.optimization_barrier(partial_value.astype(jnp.bfloat16))
        .astype(jnp.float32)
        .astype(jnp.bfloat16),
        "tp",
        scatter_dimension=0,
        tiled=True,
    )
    returned = lax.all_to_all(
        summed.reshape(expert_count, capacity, D), "sp", split_axis=0, concat_axis=0, tiled=True
    )
    picked = jnp.dot(
        picker, returned.reshape(slot_total, D), preferred_element_type=jnp.float32
    ).reshape(row_count, top_count, D)
    mixture = jnp.sum(picked * assignment_share[:, :, None], axis=1)
    return (hidden_float + mixture).astype(jnp.bfloat16)


def solution(mesh):
    placed = (
        P(("grp", "sp", "tp"), None),
        P(("grp", "sp"), "tp"),
        P(("grp", "sp"), "tp"),
        P(("grp", "sp"), "tp"),
        P(("grp", "sp"), "tp"),
        P(None, "tp"),
        P(None, "tp"),
        P(("grp", "sp"), "tp"),
        P(("grp", "sp"), "tp"),
        P(("grp", "sp"), "tp"),
        P("tp"),
        P("tp", None),
        P(),
        P(("grp", "sp", "tp"), None),
        P(("grp", "sp", "tp"), None),
        P("sp", None, "tp"),
        P("sp", None, "tp"),
        P("sp", "tp", None),
    )
    return jax.shard_map(
        local, mesh=mesh, in_specs=placed, out_specs=P(("grp", "sp", "tp"), None), check_vma=False
    )
```

profile of v0, /device:TPU:0, one launch (start us, length us, event | category | flops | bytes accessed | tf_op | source)
XLA Modules:
  0.0 321.0 jit_solution(10407767026930307422)
XLA Ops:
  21.1 15.1 %all-gather.3 = bf16[8,64,128]{2,1,0:T(8,128)(2,1)S(1)} all-gather(bf16[2,64,128]{2,1,0:T(8,128)(2,1)S(1)} %convolution_convert_fusion.2), channel_id=5, replica_groups=mesh['grp'=2,'sp'=4,'tp'=4] {'sp'}, dimensions={0}, use_global_device_ids=true | all-gather | bytes 163840 | tf_op jit(solution)/shard_map/all_gather | solution.py:21
  39.0 13.5 %all-gather.2 = bf16[512,128]{1,0:T(8,128)(2,1)S(1)} all-gather(bf16[128,128]{1,0:T(8,128)(2,1)S(1)} %convolution_convert_fusion.3), channel_id=4, replica_groups=mesh['grp'=2,'sp'=4,'tp'=4] {'sp'}, dimensions={0}, use_global_device_ids=true | all-gather | bytes 163840 | tf_op jit(solution)/shard_map/all_gather | solution.py:21
  52.5 11.2 %all_gather.49 = bf16[4,1,128]{2,1,0:T(2,128)(2,1)S(1)} all-gather(bf16[1,1,128]{2,1,0:T(2,128)(2,1)} %slice.116), channel_id=1, replica_groups=mesh['grp'=2,'sp'=4,'tp'=4] {'sp'}, dimensions={0}, use_global_device_ids=true | all-gather | bytes 1280 | tf_op jit(solution)/shard_map/all_gather | solution.py:21
  63.7 7.7 %all_gather.52 = bf16[4,2,64]{2,1,0:T(2,128)(2,1)S(1)} all-gather(bf16[1,2,64]{2,1,0:T(2,128)(2,1)} %slice.114), channel_id=1, replica_groups=mesh['grp'=2,'sp'=4,'tp'=4] {'sp'}, dimensions={0}, use_global_device_ids=true | all-gather | bytes 1280 | tf_op jit(solution)/shard_map/all_gather | solution.py:21
  72.3 6.6 %while.91 = (s32[]{:T(128)}, f32[1,128,128]{2,1,0:T(8,128)S(1)}, f32[2,1,64,128]{3,2,1,0:T(8,128)S(1)}, f32[2,1,64,128]{3,2,1,0:T(8,128)S(1)}, f32[2,1,64,128]{3...) while((s32[]{:T(128)}, f32[1,128,128]{2,1,0:T(8,128)S(1)}, ...), condition=%wide.region_13.14_spmd.clone.clone, body=%wide.region_11.13_spmd.clone.clone.sunk | while | flops 35184640 | bytes 5108845 | solution.py:82
  76.4 1.7 fusion.233
  80.0 13.4 %all-gather = bf16[512,128]{1,0:T(8,128)(2,1)S(1)} all-gather(bf16[128,128]{1,0:T(8,128)(2,1)S(1)} %convolution_convert_fusion.5), channel_id=2, replica_groups=mesh['grp'=2,'sp'=4,'tp'=4] {'sp'}, dimensions={0}, use_global_device_ids=true | all-gather | bytes 163840 | tf_op jit(solution)/shard_map/all_gather | solution.py:21
  93.7 13.4 %all-gather.1 = bf16[8,64,128]{2,1,0:T(8,128)(2,1)S(1)} all-gather(bf16[2,64,128]{2,1,0:T(8,128)(2,1)S(1)} %convolution_convert_fusion.4), channel_id=3, replica_groups=mesh['grp'=2,'sp'=4,'tp'=4] {'sp'}, dimensions={0}, use_global_device_ids=true | all-gather | bytes 163840 | tf_op jit(solution)/shard_map/all_gather | solution.py:21
  107.0 9.3 %all_gather.43 = bf16[4,1,128]{2,1,0:T(2,128)(2,1)S(1)} all-gather(bf16[1,1,128]{2,1,0:T(2,128)(2,1)S(1)} %copy-done.16), channel_id=1, replica_groups=mesh['grp'=2,'sp'=4,'tp'=4] {'sp'}, dimensions={0}, use_global_device_ids=true | all-gather | bytes 1280 | tf_op jit(solution)/shard_map/all_gather | solution.py:21
  116.3 7.8 %all_gather.46 = bf16[4,2,64]{2,1,0:T(2,128)(2,1)S(1)} all-gather(bf16[1,2,64]{2,1,0:T(2,128)(2,1)S(1)} %copy-done.17), channel_id=1, replica_groups=mesh['grp'=2,'sp'=4,'tp'=4] {'sp'}, dimensions={0}, use_global_device_ids=true | all-gather | bytes 1280 | tf_op jit(solution)/shard_map/all_gather | solution.py:21
  124.5 6.6 %while.90 = (s32[]{:T(128)}, f32[1,128,128]{2,1,0:T(8,128)S(1)}, f32[2,1,64,128]{3,2,1,0:T(8,128)S(1)}, f32[2,1,64,128]{3,2,1,0:T(8,128)S(1)}, f32[2,1,64,128]{3...) while((s32[]{:T(128)}, f32[1,128,128]{2,1,0:T(8,128)S(1)}, ...), condition=%wide.region_6.7_spmd.clone.clone, body=%wide.region_4.6_spmd.clone.clone.sunk | while | flops 35184640 | bytes 5108845 | solution.py:82
  131.5 24.4 %while.93 = (s32[]{:T(128)}, f32[2,64,128]{2,1,0:T(8,128)S(1)}, f32[2,2,64,128]{3,2,0,1:T(8,128)S(1)}, f32[2,2,64,64]{3,2,1,0:T(8,128)S(1)}, f32[2,2,64,64]{3,2,...) while((s32[]{:T(128)}, f32[2,64,128]{2,1,0:T(8,128)S(1)}, ...), condition=%wide.region_19.20_spmd.clone.clone, body=%wide.region_17.19_spmd.clone.clone.sunk | while | flops 41480192 | bytes 9778289 | solution.py:82
  131.7 2.5 exponential_select_fusion.11
  134.1 5.6 %copy.441 = f32[2,64,64,64]{1,2,3,0:T(8,128)} copy(f32[2,64,64,64]{3,2,1,0:T(8,128)} %exponential_select_fusion.11) | data formatting | bytes 4194304 | tf_op jit(solution)/shard_map/while
  139.9 2.9 fusion.249
  143.9 2.5 exponential_select_fusion.11
  146.3 5.6 %copy.441 = f32[2,64,64,64]{1,2,3,0:T(8,128)} copy(f32[2,64,64,64]{3,2,1,0:T(8,128)} %exponential_select_fusion.11) | data formatting | bytes 4194304 | tf_op jit(solution)/shard_map/while
  152.1 2.9 fusion.249
  156.5 24.3 %while.92 = (s32[]{:T(128)}, f32[2,64,128]{2,1,0:T(8,128)S(1)}, f32[2,2,64,128]{3,2,0,1:T(8,128)S(1)}, f32[2,2,64,64]{3,2,1,0:T(8,128)S(1)}, f32[2,2,64,64]{3,2,...) while((s32[]{:T(128)}, f32[2,64,128]{2,1,0:T(8,128)S(1)}, ...), condition=%wide.region_16.17_spmd.clone.clone, body=%wide.region_14.16_spmd.clone.clone.sunk | while | flops 41480192 | bytes 9779309 | solution.py:82
  156.7 2.5 exponential_select_fusion.10
  159.1 5.6 %copy.438 = f32[2,64,64,64]{1,2,3,0:T(8,128)} copy(f32[2,64,64,64]{3,2,1,0:T(8,128)} %exponential_select_fusion.10) | data formatting | bytes 4194304 | tf_op jit(solution)/shard_map/while
  164.9 2.9 fusion.241
  168.8 2.5 exponential_select_fusion.10
  171.2 5.6 %copy.438 = f32[2,64,64,64]{1,2,3,0:T(8,128)} copy(f32[2,64,64,64]{3,2,1,0:T(8,128)} %exponential_select_fusion.10) | data formatting | bytes 4194304 | tf_op jit(solution)/shard_map/while
  177.1 2.9 fusion.241
  183.6 21.2 %reduce-scatter.3.cloned.1.call-done = bf16[32,2048]{1,0:T(8,128)(2,1)} async-done(((bf16[128,2048]{1,0:T(8,128)(2,1)}), bf16[32,2048]{1,0:T(8,128)(2,1)}) %reduce-scatter.3.cloned.1.call-update) | async-done | bytes 131088 | tf_op jit(solution)/shard_map/reduce_scatter | solution.py:238
  207.1 18.8 %all_to_all.10 = bf16[4,32,2048]{2,1,0:T(8,128)(2,1)} all-to-all(bf16[4,32,2048]{2,1,0:T(8,128)(2,1)S(1)} %bitcast.547), channel_id=1, replica_groups=mesh['grp'=2,'sp'=4,'tp'=4] {'sp'}, dimensions={0} | all-to-all | bytes 1048576 | tf_op jit(solution)/shard_map/all_to_all | solution.py:275
  226.2 20.6 %all-gather.6.cloned.1.call-done = bf16[16,32,2048]{2,1,0:T(8,128)(2,1)} async-done(((bf16[4,32,2048]{2,1,0:T(8,128)(2,1)}), bf16[16,32,2048]{2,1,0:T(8,128)(2,1)}) %all-gather.6.cloned.1.call-update) | async-done | bytes 2097168 | tf_op jit(solution)/shard_map/all_gather | solution.py:274
  246.8 6.3 %fusion.102 = f32[512,896]{1,0:T(8,128)} fusion(bf16[512,2048]{1,0:T(8,128)(2,1)} %bitcast.584, bf16[1,2048,896]{2,1,0:T(8,128)(2,1)} %param.45), kind=kOutput, calls=%fused_computation.146 | convolution fusion | flops 1879048192 | bytes 7602176 | tf_op jit(solution)/shard_map/dot_general | solution.py:281
  253.1 10.1 %fusion.104 = bf16[512,2048]{1,0:T(8,128)(2,1)} fusion(bf16[1,896,2048]{2,1,0:T(8,128)(2,1)} %param.47, f32[512,896]{1,0:T(8,128)} %fusion.102, bf16[512,2048]{1,0:T(8,128)(2,1)} %bitcast.585, bf16[1,2048,896]{2,1,0:T(8,128)(2,1)} %param.46), kind=kOutput, calls=%fused_computation.148 | convolution fusion | flops 3761897472 | bytes 13369344 | tf_op jit(solution)/shard_map/dot_general | solution.py:291
  263.2 31.3 %reduce-scatter.5.cloned.1.call-done = bf16[128,2048]{1,0:T(8,128)(2,1)} async-done(((bf16[512,2048]{1,0:T(8,128)(2,1)}), bf16[128,2048]{1,0:T(8,128)(2,1)}) %reduce-scatter.5.cloned.1.call-update) | async-done | bytes 524304 | tf_op jit(solution)/shard_map/reduce_scatter | solution.py:294
  294.5 18.9 %all_to_all.11 = bf16[4,32,2048]{2,1,0:T(8,128)(2,1)S(1)} all-to-all(bf16[4,32,2048]{2,1,0:T(8,128)(2,1)} %bitcast.565), channel_id=1, replica_groups=mesh['grp'=2,'sp'=4,'tp'=4] {'sp'}, dimensions={0} | all-to-all | bytes 1048576 | tf_op jit(solution)/shard_map/all_to_all | solution.py:302
  (248 shorter events, 43.2 us)
Async XLA Ops:
  6.5 174.9 %copy-start = (bf16[384,2048]{1,0:T(8,128)(2,1)S(1)}, bf16[384,2048]{1,0:T(8,128)(2,1)}, u32[]{:S(2)}) copy-start(bf16[384,2048]{1,0:T(8,128)(2,1)} %param.41) | copy-start | bytes 4718596
  6.5 12.7 %copy-start.9 = (bf16[128,128]{1,0:T(8,128)(2,1)S(1)}, bf16[128,128]{1,0:T(8,128)(2,1)}, u32[]{:S(2)}) copy-start(bf16[128,128]{1,0:T(8,128)(2,1)} %param.32) | copy-start | bytes 98308
  6.5 198.2 %reduce-scatter.3.cloned.1.call-start = ((), (), s32[]{:S(2)}) async-start(), calls=%async_computation.4 | async-start | bytes 655360 | tf_op jit(solution)/shard_map/reduce_scatter | solution.py:238
  10.5 4.4 %copy-start.13 = (f32[128]{0:T(128)}, f32[128]{0:T(128)S(1)}, u32[]{:S(2)}) copy-start(f32[128]{0:T(128)S(1)} %get-tuple-element.948) | copy-start | bytes 1540
  16.3 1.2 copy-start.6
  20.3 51.9 %copy-start.8 = (bf16[128,128]{1,0:T(8,128)(2,1)S(1)}, bf16[128,128]{1,0:T(8,128)(2,1)}, u32[]{:S(2)}) copy-start(bf16[128,128]{1,0:T(8,128)(2,1)} %param.31) | copy-start | bytes 98308
  72.3 6.7 %copy-start.7 = (f32[128,1,128]{2,1,0:T(1,128)S(1)}, f32[128,1,128]{2,1,0:T(1,128)}, u32[]{:S(2)}) copy-start(f32[128,1,128]{2,1,0:T(1,128)} %copy-done.6) | copy-start | bytes 196612
  72.3 6.7 %copy-start.14 = (f32[128]{0:T(128)S(1)}, f32[128]{0:T(128)}, u32[]{:S(2)}) copy-start(f32[128]{0:T(128)} %copy-done.13) | copy-start | bytes 1540
  72.3 6.7 %copy-start.18 = (f32[128]{0:T(128)S(1)}, f32[128]{0:T(128)}, u32[]{:S(2)}) copy-start(f32[128]{0:T(128)} %slice_bitcast_fusion.10) | copy-start | bytes 1540
  72.3 34.7 %copy-start.16 = (bf16[1,1,128]{2,1,0:T(2,128)(2,1)S(1)}, bf16[1,1,128]{2,1,0:T(2,128)(2,1)}, u32[]{:S(2)}) copy-start(bf16[1,1,128]{2,1,0:T(2,128)(2,1)} %slice.117) | copy-start | bytes 772
  72.3 44.0 %copy-start.17 = (bf16[1,2,64]{2,1,0:T(2,128)(2,1)S(1)}, bf16[1,2,64]{2,1,0:T(2,128)(2,1)}, u32[]{:S(2)}) copy-start(bf16[1,2,64]{2,1,0:T(2,128)(2,1)} %slice.115) | copy-start | bytes 772
  78.9 45.5 %copy-start.4 = (f32[128,1,1,128]{0,3,2,1:T(8,128)S(1)}, f32[128,1,1,128]{0,3,2,1:T(8,128)}, u32[]{:S(2)}) copy-start(f32[128,1,1,128]{0,3,2,1:T(8,128)} %slice.82) | copy-start | bytes 196612
  124.5 6.7 %copy-start.3 = (f32[128,128]{0,1:T(8,128)S(1)}, f32[128,128]{0,1:T(8,128)}, u32[]{:S(2)}) copy-start(f32[128,128]{0,1:T(8,128)} %convert_element_type.202) | copy-start | bytes 196612
  156.5 24.7 %copy-start.5 = (bf16[128,384]{1,0:T(8,128)(2,1)S(1)}, bf16[128,384]{1,0:T(8,128)(2,1)}, u32[]{:S(2)}) copy-start(bf16[128,384]{1,0:T(8,128)(2,1)} %param.38) | copy-start | bytes 294916
  156.5 24.8 %copy-start.12 = (f32[384]{0:T(512)S(1)}, f32[384]{0:T(512)}, u32[]{:S(2)}) copy-start(f32[384]{0:T(512)} %param.40) | copy-start | bytes 4612
  180.8 1.9 copy-start.11
  180.8 23.9 %copy-start.1 = (bf16[32,2048]{1,0:T(8,128)(2,1)S(1)}, bf16[32,2048]{1,0:T(8,128)(2,1)}, u32[]{:S(2)}) copy-start(bf16[32,2048]{1,0:T(8,128)(2,1)} %param.30) | copy-start | bytes 393220
  181.0 24.8 %copy-start.10 = (f32[2048]{0:T(1024)S(1)}, f32[2048]{0:T(1024)}, u32[]{:S(2)}) copy-start(f32[2048]{0:T(1024)} %param.42) | copy-start | bytes 24580
  182.7 64.1 %all-gather.6.cloned.1.call-start = ((), (), s32[]{:S(2)}) async-start(), calls=%async_computation.5 | async-start | bytes 2621440 | tf_op jit(solution)/shard_map/all_gather | solution.py:274
  226.0 68.6 %reduce-scatter.5.cloned.1.call-start = ((), (), s32[]{:S(2)}) async-start(), calls=%async_computation.6 | async-start | bytes 2621440 | tf_op jit(solution)/shard_map/reduce_scatter | solution.py:294
  263.2 50.3 %copy-start.15 = (f32[32,2]{0,1:T(2,128)S(1)}, f32[32,2]{0,1:T(2,128)}, u32[]{:S(2)}) copy-start(f32[32,2]{0,1:T(2,128)} %param.44) | copy-start | bytes 772
  263.2 50.6 %copy-start.2 = (bf16[32,2048]{1,0:T(8,128)(2,1)S(1)}, bf16[32,2048]{1,0:T(8,128)(2,1)}, u32[]{:S(2)}) copy-start(bf16[32,2048]{1,0:T(8,128)(2,1)} %reduce-scatter.3.cloned.1.call-done) | copy-start | bytes 393220
Sparse Core Ops, SparseCore 0:
  182.8 21.8 reduce-scatter.2
  226.1 20.6 all-gather.5
  263.3 31.1 reduce-scatter.4
where the time goes:
time: 322 us; the launch traced here: 321 us
  blocking collectives  129 us (40%)
  waiting for transfers between devices  73.1 us (23%)
  other arithmetic  39.2 us (12%)
  local copies, waits for them, and re-layouts  36.4 us (11%)
  matrix products  28 us (9%)
  between operations  13.8 us (4%)
    all_gather x8, blocking collectives, carried_in(): lax.all_gather(a.astype(kind), axis)  91.4 us
    reduce_scatter x1, waiting for transfers between devices, local(): lax.psum_scatter(lax.optimization_barrier(partial_value.astype(jnp.bfloat...  31.3 us
    while x4, local copies, waits for them, and re-layouts  22.4 us
    reduce_scatter x1, waiting for transfers between devices, local(): lax.psum_scatter(jnp.dot(mixed_heads, result_mapping_matrix, preferred_el...  21.2 us
    all_gather x1, waiting for transfers between devices, local(): lax.all_gather(lax.all_to_all(outgoing, 'sp', split_axis=0, concat_axis=0...  20.6 us
    all_to_all x1, blocking collectives, local(): lax.all_to_all(summed.reshape(expert_count, capacity, D), 'sp', split_axi...  18.9 us
    all_to_all x1, blocking collectives, local(): lax.all_to_all(outgoing, 'sp', split_axis=0, concat_axis=0, tiled=True)  18.8 us
    dot_general x8, other arithmetic, advance(): jnp.einsum('htd,hsd,htsd->hts', query_block, key_block, weight, precision...  18.3 us
  transfers between devices with their start and end apart: 3, of which 3 were waited for; matrix products, arithmetic and copies ran while one was open for 0% of the time, Pallas kernels for 0%

commit v1 on v0

v1 whole, which is shorter than its diff:
```python
import functools

import jax
import jax.numpy as jnp
from jax import lax
from jax.experimental import pallas as pl
from jax.experimental.pallas import tpu as pltpu
from jax.sharding import PartitionSpec as P

LANES = 128
NEAR = 2
EPS = 1e-06
F32 = jnp.float32
BF16 = jnp.bfloat16


def mm(a, b, ca=1, cb=0):
    return lax.dot_general(a, b, (((ca,), (cb,)), ((), ())), preferred_element_type=F32)


def kernel(
    n_sp,
    n_tp,
    cap,
    capp,
    skip_ref,
    wq_ref,
    nq_ref,
    wf_ref,
    nf_ref,
    wl_ref,
    nl_ref,
    v_ref,
    gate_ref,
    spk_ref,
    chs_ref,
    wo_hbm,
    nsc_ref,
    asg_ref,
    shr_ref,
    wg_hbm,
    wu_hbm,
    wd_hbm,
    out_ref,
    wo,
    wg,
    wu,
    wd,
    st_out,
    st_in,
    y_s,
    rs_out,
    rs_in,
    hid_s,
    disp,
    xin,
    part,
    nr_in,
    fr_out,
    fr_in,
    fin,
    ret,
    wsem,
    st_ss,
    st_rs,
    rs_ss,
    rs_rs,
    z_ss,
    far_ss,
    near_ss,
    ag_rs,
    nr_ss,
    nr_rs,
    fr_ss,
    fr_rs,
    ret_ss,
    ret_rs,
):
    sp = lax.axis_index("sp")
    tp = lax.axis_index("tp")
    n_hi = n_tp // NEAR
    hi = tp // NEAR
    near = tp + 1 - 2 * (tp % NEAR)
    near_lo = near % NEAR
    lo = tp % NEAR
    rows = skip_ref.shape[0]
    L = wq_ref.shape[0]
    H = L // 2
    group = n_tp * capp

    def al(i):
        return pl.multiple_of(i * capp, capp)

    weights = [
        pltpu.make_async_copy(wo_hbm, wo, wsem.at[0]),
        pltpu.make_async_copy(wg_hbm.at[0], wg, wsem.at[1]),
        pltpu.make_async_copy(wu_hbm.at[0], wu, wsem.at[2]),
        pltpu.make_async_copy(wd_hbm.at[0], wd, wsem.at[3]),
    ]
    for w in weights:
        w.start()

    barrier = pltpu.get_barrier_semaphore()
    for o in range(1, n_sp):
        pl.semaphore_signal(barrier, inc=1, device_id={"sp": (sp + o) % n_sp})
    for o in range(1, n_tp):
        pl.semaphore_signal(barrier, inc=1, device_id={"tp": (tp + o) % n_tp})

    lane = lax.broadcasted_iota(jnp.int32, (1, LANES), 1)
    first = lane < LANES // 2
    spk = spk_ref[...]
    spike = jnp.concatenate(
        [
            jnp.broadcast_to(spk[:, 0:1], (L, LANES)),
            jnp.where(first, spk[:, 1:2], spk[:, 2:3]),
        ],
        axis=1,
    )
    forget = jnp.concatenate([wf_ref[...], nf_ref[...]], axis=1).astype(F32)
    start = 1.0 / (1.0 + jnp.exp(forget))
    wq = wq_ref[...].astype(F32)
    nq = nq_ref[...].astype(F32)
    q = jnp.concatenate(
        [
            wq / (1.0 + jnp.exp(-wq)) * LANES**-0.5,
            nq / (1.0 + jnp.exp(-nq)) * (LANES // 2) ** -0.5,
        ],
        axis=1,
    )
    leak = jnp.concatenate([wl_ref[...], nl_ref[...]], axis=1)
    t_i = lax.broadcasted_iota(jnp.int32, (L, L), 0)
    s_i = lax.broadcasted_iota(jnp.int32, (L, L), 1)
    row = lax.broadcasted_iota(jnp.int32, (L, 1), 0)
    past = s_i <= t_i
    later = s_i >= t_i
    same = (t_i < H) == (s_i < H)
    v = v_ref[...]
    vs = [v[:, h * LANES : (h + 1) * LANES] for h in range(3)]
    ks, runs = [], []
    for d in range(2):
        k = leak[d : d + 1, :] * start
        a = jnp.log(1.0 - k) + spike
        tri = (past if d == 0 else later).astype(F32)
        run = lax.dot_general(
            tri,
            a,
            (((1,), (0,)), ((), ())),
            preferred_element_type=F32,
            precision=lax.Precision.HIGHEST,
        )
        total = run[L - 1 : L, :] if d == 0 else run[0:1, :]
        kk = (k * jnp.exp(total - run)).astype(BF16)
        wide = mm(vs[0], kk[:, :LANES], 0, 0)
        slim = jnp.where(first, mm(vs[1], kk[:, LANES:], 0, 0), mm(vs[2], kk[:, LANES:], 0, 0))
        st_out[d, :LANES, :] = jnp.concatenate([wide, slim], axis=1).astype(BF16)
        st_out[d, LANES:, :] = jnp.broadcast_to(
            total, (st_out.shape[1] - LANES, 2 * LANES)
        ).astype(BF16)
        ks.append(k)
        runs.append(run)

    pl.semaphore_wait(barrier, n_sp + n_tp - 2)

    def st_copy(o):
        dest = (sp + o) % n_sp
        way = (sp + o) // n_sp
        return pltpu.make_async_remote_copy(
            src_ref=st_out.at[way],
            dst_ref=st_in.at[sp],
            send_sem=st_ss.at[o],
            recv_sem=st_rs.at[sp],
            device_id={"sp": dest},
        )

    for o in range(1, n_sp):
        st_copy(o).start()

    outs = []
    scores = [None, None, None]
    for d in range(2):
        k, run = ks[d], runs[d]
        mid = jnp.where(row < H, run[H // 2 - 1 : H // 2, :], run[H + H // 2 - 1 : H + H // 2, :])
        edge = run[H - 1 : H, :] if d == 0 else run[H : H + 1, :]
        q_in = q * jnp.exp(run - mid)
        k_in = (k * jnp.exp(mid - run)).astype(BF16)
        q_off = q * jnp.exp(jnp.minimum(run - edge, 0.0))
        k_off = (k * jnp.exp(jnp.minimum(edge - run, 0.0))).astype(BF16)
        keep_in = same & (past if d == 0 else later)
        keep_off = ((t_i >= H) & (s_i < H)) if d == 0 else ((t_i < H) & (s_i >= H))
        for h in range(3):
            at = slice(0, LANES) if h == 0 else slice(LANES, 2 * LANES)
            qi, qo = q_in[:, at], q_off[:, at]
            if h > 0:
                mine = first if h == 1 else ~first
                qi, qo = jnp.where(mine, qi, 0.0), jnp.where(mine, qo, 0.0)
            part_in = jnp.where(keep_in, mm(qi.astype(BF16), k_in[:, at], 1, 1), 0.0)
            part_off = jnp.where(keep_off, mm(qo.astype(BF16), k_off[:, at], 1, 1), 0.0)
            both = part_in + part_off
            scores[h] = both if d == 0 else scores[h] + both
    for h in range(3):
        outs.append(mm(scores[h].astype(BF16), vs[h]))

    def take(src, state):
        pltpu.make_async_remote_copy(
            src_ref=st_out.at[0],
            dst_ref=st_in.at[src],
            send_sem=st_ss.at[0],
            recv_sem=st_rs.at[src],
            device_id={"sp": (sp + 1) % n_sp},
        ).wait_recv()
        got = st_in[src].astype(F32)
        return state * jnp.exp(got[LANES : LANES + 1, :]) + got[:LANES, :]

    zero = jnp.zeros((LANES, 2 * LANES), F32)
    ahead = lax.fori_loop(0, sp, take, zero)
    behind = lax.fori_loop(0, n_sp - 1 - sp, lambda i, s: take(n_sp - 1 - i, s), zero)
    for d, state in enumerate((ahead, behind)):
        state = state.astype(BF16)
        qd = q * jnp.exp(runs[d])
        for h in range(3):
            at = slice(0, LANES) if h == 0 else slice(LANES, 2 * LANES)
            qh = qd[:, at]
            if h > 0:
                qh = jnp.where(first if h == 1 else ~first, qh, 0.0)
            outs[h] = outs[h] + mm(qh.astype(BF16), state[:, at], 1, 1)
    g = gate_ref[...].astype(F32)
    g = g / (1.0 + jnp.exp(-g)) * chs_ref[...]
    for h in range(3):
        at = slice(h * LANES, (h + 1) * LANES)
        o_h = outs[h]
        o_h = o_h * lax.rsqrt(jnp.mean(o_h * o_h, axis=1, keepdims=True) + EPS)
        y_s[:, at] = (o_h * g[:, at]).astype(BF16)

    weights[0].wait()
    y = y_s[...]
    D = wo.shape[1]
    step = D // 4
    for c in range(4):
        rs_out[:, c * step : (c + 1) * step] = mm(y, wo[:, c * step : (c + 1) * step]).astype(BF16)

    def rs_copy(o):
        dest = (tp + o) % n_tp
        return pltpu.make_async_remote_copy(
            src_ref=rs_out.at[pl.ds(pl.multiple_of(dest * rows, rows), rows)],
            dst_ref=rs_in.at[o - 1],
            send_sem=rs_ss.at[o - 1],
            recv_sem=rs_rs.at[o - 1],
            device_id={"tp": dest},
        )

    for o in range(1, n_tp):
        rs_copy(o).start()

    n_slot = n_sp * capp
    slot = lax.broadcasted_iota(jnp.int32, (1, n_slot), 1)
    expert = jnp.zeros((1, n_slot), jnp.int32)
    for e in range(1, n_sp):
        expert = expert + (slot >= e * capp).astype(jnp.int32)
    place = (slot - expert * capp).astype(F32)
    asg = asg_ref[...]
    shr = shr_ref[...]
    named = jnp.zeros((rows, n_slot), F32)
    share = jnp.zeros((rows, n_slot), F32)
    for c in range(asg.shape[1]):
        hit = asg[:, c : c + 1] == expert
        named = jnp.where(hit, 1.0, named)
        share = jnp.where(hit, shr[:, c : c + 1], share)
    before = (
        lax.broadcasted_iota(jnp.int32, (rows, rows), 1)
        < lax.broadcasted_iota(jnp.int32, (rows, rows), 0)
    ).astype(BF16)
    count = mm(before, named.astype(BF16))
    picked = jnp.where(count == place, named, 0.0)
    comb = picked * share
    comb_hi = comb.astype(BF16)
    comb_lo = (comb - comb_hi.astype(F32)).astype(BF16)

    total = skip_ref[...].astype(F32) + rs_out[pl.ds(pl.multiple_of(tp * rows, rows), rows), :].astype(F32)
    for o in range(1, n_tp):
        rs_copy(o).wait_recv()
        total = total + rs_in[o - 1].astype(F32)
    hid = total.astype(BF16)
    hid_s[...] = hid
    hf = hid.astype(F32)
    normed = (
        hf * lax.rsqrt(jnp.mean(hf * hf, axis=1, keepdims=True) + EPS) * nsc_ref[...]
    ).astype(BF16)
    disp[...] = mm(picked.astype(BF16), normed, 0, 0).astype(BF16)

    def chunk(src, t):
        return al(src * n_tp + t)

    def z_copy(o):
        dest = (sp + o) % n_sp
        return pltpu.make_async_remote_copy(
            src_ref=disp.at[pl.ds(al(dest), capp)],
            dst_ref=xin.at[pl.ds(chunk(sp, tp), capp)],
            send_sem=z_ss.at[o],
            recv_sem=ag_rs.at[sp, tp],
            device_id={"sp": dest},
        )

    for o in range(1, n_sp):
        z_copy(o).start()
    xin[pl.ds(chunk(sp, tp), capp), :] = disp[pl.ds(al(sp), capp), :]

    def source(i):
        return (sp + i) % n_sp

    def tp_copy(src, t, sem, dest):
        return pltpu.make_async_remote_copy(
            src_ref=xin.at[pl.ds(chunk(src, t), capp)],
            dst_ref=xin.at[pl.ds(chunk(src, t), capp)],
            send_sem=sem,
            recv_sem=ag_rs.at[src, t],
            device_id={"tp": dest},
        )

    def far_copy(i, h):
        return tp_copy(source(i), tp, far_ss.at[i, h], (tp + NEAR * h) % n_tp)

    def near_copy(i, h):
        return tp_copy(source(i), (tp + NEAR * h) % n_tp, near_ss.at[i, h], near)

    def arrived(i, t):
        tp_copy(source(i), t, near_ss.at[i, 0], near).wait_recv()

    def spread(i):
        for h in range(1, n_hi):
            far_copy(i, h).start()
        near_copy(i, 0).start()

    def relay(i):
        for h in range(1, n_hi):
            arrived(i, (tp + NEAR * h) % n_tp)
            near_copy(i, h).start()

    def nr_copy(i, h):
        src = source(i)
        return pltpu.make_async_remote_copy(
            src_ref=part.at[pl.ds(chunk(src, h * NEAR + near_lo), capp)],
            dst_ref=nr_in.at[pl.ds(al(src * n_hi + h), capp)],
            send_sem=nr_ss.at[i, h],
            recv_sem=nr_rs.at[src, h],
            device_id={"tp": near},
        )

    def fr_copy(i, o):
        src = source(i)
        h = (hi + o) % n_hi
        return pltpu.make_async_remote_copy(
            src_ref=fr_out.at[pl.ds(al(src * n_hi + h), capp)],
            dst_ref=fr_in.at[pl.ds(al(src * n_hi + o), capp)],
            send_sem=fr_ss.at[i, o],
            recv_sem=fr_rs.at[src, o],
            device_id={"tp": (tp + NEAR * o) % n_tp},
        )

    def ret_copy(i):
        src = source(i)
        return pltpu.make_async_remote_copy(
            src_ref=fin.at[pl.ds(al(src), capp)],
            dst_ref=ret.at[pl.ds(al(sp), capp)],
            send_sem=ret_ss.at[i],
            recv_sem=ret_rs.at[sp],
            device_id={"sp": src},
        )

    def ffn(i):
        src = source(i)
        for h in range(n_hi):
            arrived(i, (near + NEAR * h) % n_tp)
        at = pl.multiple_of(src * group, group)
        x = xin[pl.ds(at, group), :]
        gp = mm(x, wg[...])
        up = mm(x, wu[...])
        act = (gp / (1.0 + jnp.exp(-gp)) * up).astype(BF16)
        for c in range(4):
            part[pl.ds(at, group), c * step : (c + 1) * step] = mm(
                act, wd[:, c * step : (c + 1) * step]
            ).astype(BF16)
        for h in range(n_hi):
            nr_copy(i, h).start()

    def near_sum(i):
        src = source(i)
        for o in range(1, n_hi + 1):
            h = (hi + o) % n_hi
            nr_copy(i, h).wait_recv()
            slot_at = pl.ds(al(src * n_hi + h), capp)
            fr_out[slot_at, :] = (
                part[pl.ds(chunk(src, h * NEAR + lo), capp), :].astype(F32)
                + nr_in[slot_at, :].astype(F32)
            ).astype(BF16)
            if o < n_hi:
                fr_copy(i, o).start()

    def far_sum(i):
        src = source(i)
        acc = fr_out[pl.ds(al(src * n_hi + hi), capp), :].astype(F32)
        for o in range(1, n_hi):
            fr_copy(i, o).wait_recv()
            acc = acc + fr_in[pl.ds(al(src * n_hi + o), capp), :].astype(F32)
        fin[pl.ds(al(src), capp), :] = acc.astype(BF16)

    spread(0)
    relay(0)
    for w in weights[1:]:
        w.wait()

    def z_arrived(i):
        src = source(i)
        pltpu.make_async_remote_copy(
            src_ref=disp.at[pl.ds(0, capp)],
            dst_ref=xin.at[pl.ds(chunk(src, tp), capp)],
            send_sem=z_ss.at[0],
            recv_sem=ag_rs.at[src, tp],
            device_id={"sp": (sp + 1) % n_sp},
        ).wait_recv()

    if n_sp > 1:
        z_arrived(1)
        spread(1)

    def body(i, carry):
        @pl.when(i < n_sp)
        def _():
            ffn(i)

        @pl.when(i + 1 < n_sp)
        def _():
            relay(i + 1)

        @pl.when(i + 2 < n_sp)
        def _():
            z_arrived(i + 2)
            spread(i + 2)

        @pl.when((i >= 1) & (i <= n_sp))
        def _():
            near_sum(i - 1)

        @pl.when(i >= 2)
        def _():
            far_sum(i - 2)

        @pl.when(i >= 3)
        def _():
            ret_copy(i - 2).start()

        return carry

    lax.fori_loop(0, n_sp + 2, body, 0)

    ret[pl.ds(al(sp), capp), :] = fin[pl.ds(al(sp), capp), :]
    for o in range(1, n_sp):
        src = (sp + o) % n_sp
        pltpu.make_async_remote_copy(
            src_ref=fin.at[pl.ds(0, capp)],
            dst_ref=ret.at[pl.ds(al(src), capp)],
            send_sem=ret_ss.at[0],
            recv_sem=ret_rs.at[src],
            device_id={"sp": src},
        ).wait_recv()
    back = ret[...]
    out_ref[...] = (hid_s[...].astype(F32) + mm(comb_hi, back) + mm(comb_lo, back)).astype(BF16)

    for o in range(1, n_sp):
        st_copy(o).wait_send()
        z_copy(o).wait_send()
        ret_copy(o).wait_send()
    for o in range(1, n_tp):
        rs_copy(o).wait_send()

    def drain(i, carry):
        for h in range(1, n_hi):
            far_copy(i, h).wait_send()
            fr_copy(i, h).wait_send()
        for h in range(n_hi):
            near_copy(i, h).wait_send()
            nr_copy(i, h).wait_send()
        return carry

    lax.fori_loop(0, n_sp, drain, 0)


def local(n_sp, n_tp, *args):
    skip, wq = args[0], args[1]
    rows, D = skip.shape
    L = wq.shape[0]
    top = args[13].shape[1]
    cap = max(2, 2 * rows * top // n_sp)
    cap = min(cap, rows)
    capp = -(-cap // 16) * 16
    n_hi = n_tp // NEAR
    de = args[15].shape[2]
    heads = args[11].shape[0]
    args = list(args)
    args[10] = args[10].reshape(1, -1)
    args[12] = args[12].reshape(1, -1)
    vm = pl.BlockSpec(memory_space=pltpu.VMEM)
    hbm = pl.BlockSpec(memory_space=pl.ANY)
    specs = [hbm if i in (11, 15, 16, 17) else vm for i in range(len(args))]
    dma = pltpu.SemaphoreType.DMA
    scratch = [
        pltpu.VMEM((heads, D), BF16),
        pltpu.VMEM((D, de), BF16),
        pltpu.VMEM((D, de), BF16),
        pltpu.VMEM((de, D), BF16),
        pltpu.VMEM((2, LANES + 16, 2 * LANES), BF16),
        pltpu.VMEM((n_sp, LANES + 16, 2 * LANES), BF16),
        pltpu.VMEM((L, heads), BF16),
        pltpu.VMEM((L, D), BF16),
        pltpu.VMEM((n_tp - 1, rows, D), BF16),
        pltpu.VMEM((rows, D), BF16),
        pltpu.VMEM((n_sp * capp, D), BF16),
        pltpu.VMEM((n_sp * n_tp * capp, D), BF16),
        pltpu.VMEM((n_sp * n_tp * capp, D), BF16),
        pltpu.VMEM((n_sp * n_hi * capp, D), BF16),
        pltpu.VMEM((n_sp * n_hi * capp, D), BF16),
        pltpu.VMEM((n_sp * n_hi * capp, D), BF16),
        pltpu.VMEM((n_sp * capp, D), BF16),
        pltpu.VMEM((n_sp * capp, D), BF16),
        dma((4,)),
        dma((n_sp,)),
        dma((n_sp,)),
        dma((n_tp - 1,)),
        dma((n_tp - 1,)),
        dma((n_sp,)),
        dma((n_sp, n_hi)),
        dma((n_sp, n_hi)),
        dma((n_sp, n_tp)),
        dma((n_sp, n_hi)),
        dma((n_sp, n_hi)),
        dma((n_sp, n_hi)),
        dma((n_sp, n_hi)),
        dma((n_sp,)),
        dma((n_sp,)),
    ]
    return pl.pallas_call(
        functools.partial(kernel, n_sp, n_tp, cap, capp),
        out_shape=jax.ShapeDtypeStruct((rows, D), BF16),
        in_specs=specs,
        out_specs=vm,
        scratch_shapes=scratch,
        compiler_params=pltpu.CompilerParams(
            collective_id=0, has_side_effects=True, vmem_limit_bytes=60 * 1024 * 1024
        ),
    )(*args)


def solution(mesh):
    placed = (
        P(("grp", "sp", "tp"), None),
        P(("grp", "sp"), "tp"),
        P(("grp", "sp"), "tp"),
        P(("grp", "sp"), "tp"),
        P(("grp", "sp"), "tp"),
        P(None, "tp"),
        P(None, "tp"),
        P(("grp", "sp"), "tp"),
        P(("grp", "sp"), "tp"),
        P(("grp", "sp"), "tp"),
        P("tp"),
        P("tp", None),
        P(),
        P(("grp", "sp", "tp"), None),
        P(("grp", "sp", "tp"), None),
        P("sp", None, "tp"),
        P("sp", None, "tp"),
        P("sp", "tp", None),
    )
    return jax.shard_map(
        functools.partial(local, mesh.shape["sp"], mesh.shape["tp"]),
        mesh=mesh,
        in_specs=placed,
        out_specs=P(("grp", "sp", "tp"), None),
        check_vma=False,
    )
```

time: 322 us -> 72.5 us (0.23)
  blocking collectives: 129 us -> 0 us
  waiting for transfers between devices: 73.1 us -> 0 us
  Pallas kernels: 0 us -> 65.4 us
  other arithmetic: 39.2 us -> 0 us
  local copies, waits for them, and re-layouts: 36.4 us -> 6.93 us
  matrix products: 28 us -> 0 us
  between operations: 13.8 us -> 0.01 us
    all_gather x8 -> x0, blocking collectives: 91.4 us -> none  [carried_in(): lax.all_gather(a.astype(kind), axis)]
    pallas_call x0 -> x1, Pallas kernels: none -> 65.4 us  [local(): pl.pallas_call(functools.partial(kernel, n_sp, n_tp, cap, capp), out_shap...]
    reduce_scatter x2 -> x0, waiting for transfers between devices: 52.5 us -> none  [the longest x1 31.3 us: local(): lax.psum_scatter(lax.optimization_barrier(partial_value.astype(jnp.bfloat...]
    all_to_all x2 -> x0, blocking collectives: 37.8 us -> none  [the longest x1 18.9 us: local(): lax.all_to_all(summed.reshape(expert_count, capacity, D), 'sp', split_axi...]
    dot_general x33 -> x0, matrix products: 28 us -> none  [the longest x1 10.1 us: local(): jnp.dot(row_block, specialist_lowering_matrix[0], preferred_element_type=...]
    while x4 -> x0, local copies, waits for them, and re-layouts: 22.4 us -> none
    all_gather x1 -> x0, waiting for transfers between devices: 20.6 us -> none  [local(): lax.all_gather(lax.all_to_all(outgoing, 'sp', split_axis=0, concat_axis=0...]
    dot_general x8 -> x0, other arithmetic: 18.3 us -> none  [advance(): jnp.einsum('htd,hsd,htsd->hts', query_block, key_block, weight, precision...]
  transfers between devices with their start and end apart: 3 -> 0, of which waited for: 3 -> 0; matrix products, arithmetic and copies ran while one was open for 0% -> 0% of each run, Pallas kernels for 0% -> 0%
where the time goes in v1:
time: 72.5 us; the launch traced here: 72.3 us
  Pallas kernels  65.4 us (90%)
  local copies, waits for them, and re-layouts  6.93 us (10%)
    pallas_call x1, Pallas kernels, local(): pl.pallas_call(functools.partial(kernel, n_sp, n_tp, cap, capp), out_shap...  65.4 us
    unnamed x4, local copies, waits for them, and re-layouts  5.69 us

profile of v1, /device:TPU:0, one launch (start us, length us, event | category | flops | bytes accessed | tf_op | source)
XLA Modules:
  0.0 72.3 jit_solution(92906295329452995)
XLA Ops:
  0.0 1.2 %reshape.6.chs_ref = f32[1,384]{1,0:T(1,128)} reshape(f32[384]{0:T(512)} %param.28) | data formatting | bytes 3072 | tf_op jit(solution)/shard_map/reshape | solution.py:499
  1.2 1.4 %copy.20.asg_ref = s32[32,2]{1,0:T(8,128)} copy(s32[32,2]{0,1:T(2,128)} %param.31) | data formatting | bytes 512 | tf_op args[13]
  2.6 1.4 %copy.21.shr_ref = f32[32,2]{1,0:T(8,128)} copy(f32[32,2]{0,1:T(2,128)} %param.32) | data formatting | bytes 512 | tf_op args[14]
  4.0 1.4 %copy.19.spk_ref = f32[128,3]{1,0:T(8,128)} copy(f32[128,3]{0,1:T(4,128)} %param.27) | data formatting | bytes 3072 | tf_op args[9]
  5.4 65.4 %shard_map.172 = bf16[32,2048]{1,0:T(8,128)(2,1)} custom-call(bf16[32,2048]{1,0:T(8,128)(2,1)} %skip_ref.1, bf16[128,128]{1,0:T(8,128)(2,1)} %wq_ref.1, bf16[128,128]{1,0:T(8,128)(2,1)} %nq_ref.1, bf16[128,128]{1,0:T(8,128)(2,1)} %wf_ref.1, bf16[128,128]{1,0:T(8,128)(2,1)} %nf_ref.1, f32[2,128]{1,0:T(2,128)} %wl_ref.1, f32[2,128]{1,0:T(2,128)} %nl_ref.1, ...), custom_call_target="tpu_custom_call" | custom-call | tf_op jit(solution)/shard_map/pallas_call | solution.py:540
  70.7 1.6 %copy.23 = bf16[32,2048]{1,0:T(8,128)(2,1)} copy(bf16[32,2048]{1,0:T(8,128)(2,1)} %shard_map.172) | data formatting | bytes 262144

commit v2 on v1

--- a/solution.py
+++ b/solution.py
@@ -87,6 +87,14 @@
     L = wq_ref.shape[0]
     H = L // 2
     group = n_tp * capp
+    dense = cap >= rows and capp == rows
+    inner = jnp.minimum(sp, n_sp - 1 - sp)
+
+    def source(i):
+        apart = (i + 1) // 2
+        pair = jnp.where(i % 2 == 1, sp - apart, sp + apart)
+        tail = jnp.where(sp == inner, sp + (i - inner), sp - (i - inner))
+        return jnp.where(i <= 2 * inner, pair, tail)
 
     def al(i):
         return pl.multiple_of(i * capp, capp)
@@ -108,14 +116,8 @@
 
     lane = lax.broadcasted_iota(jnp.int32, (1, LANES), 1)
     first = lane < LANES // 2
-    spk = spk_ref[...]
-    spike = jnp.concatenate(
-        [
-            jnp.broadcast_to(spk[:, 0:1], (L, LANES)),
-            jnp.where(first, spk[:, 1:2], spk[:, 2:3]),
-        ],
-        axis=1,
-    )
+    spk = [jnp.broadcast_to(spk_ref[h : h + 1, :], (LANES, L)).T for h in range(3)]
+    spike = jnp.concatenate([spk[0], jnp.where(first, spk[1], spk[2])], axis=1)
     forget = jnp.concatenate([wf_ref[...], nf_ref[...]], axis=1).astype(F32)
     start = 1.0 / (1.0 + jnp.exp(forget))
     wq = wq_ref[...].astype(F32)
@@ -224,7 +226,7 @@
                 qh = jnp.where(first if h == 1 else ~first, qh, 0.0)
             outs[h] = outs[h] + mm(qh.astype(BF16), state[:, at], 1, 1)
     g = gate_ref[...].astype(F32)
-    g = g / (1.0 + jnp.exp(-g)) * chs_ref[...]
+    g = g / (1.0 + jnp.exp(-g)) * chs_ref[...].reshape(1, -1)
     for h in range(3):
         at = slice(h * LANES, (h + 1) * LANES)
         o_h = outs[h]
@@ -252,24 +254,25 @@
         rs_copy(o).start()
 
     n_slot = n_sp * capp
-    slot = lax.broadcasted_iota(jnp.int32, (1, n_slot), 1)
-    expert = jnp.zeros((1, n_slot), jnp.int32)
+    slot = lax.broadcasted_iota(jnp.int32, (n_slot, 1), 0)
+    expert = jnp.zeros((n_slot, 1), jnp.int32)
     for e in range(1, n_sp):
         expert = expert + (slot >= e * capp).astype(jnp.int32)
     place = (slot - expert * capp).astype(F32)
-    asg = asg_ref[...]
-    shr = shr_ref[...]
-    named = jnp.zeros((rows, n_slot), F32)
-    share = jnp.zeros((rows, n_slot), F32)
-    for c in range(asg.shape[1]):
-        hit = asg[:, c : c + 1] == expert
+    named = jnp.zeros((n_slot, rows), F32)
+    share = jnp.zeros((n_slot, rows), F32)
+    for c in range(asg_ref.shape[0]):
+        hit = asg_ref[c : c + 1, :] == expert
         named = jnp.where(hit, 1.0, named)
-        share = jnp.where(hit, shr[:, c : c + 1], share)
+        share = jnp.where(hit, shr_ref[c : c + 1, :], share)
     before = (
-        lax.broadcasted_iota(jnp.int32, (rows, rows), 1)
-        < lax.broadcasted_iota(jnp.int32, (rows, rows), 0)
+        lax.broadcasted_iota(jnp.int32, (rows, rows), 0)
+        < lax.broadcasted_iota(jnp.int32, (rows, rows), 1)
     ).astype(BF16)
-    count = mm(before, named.astype(BF16))
+    if dense:
+        count = lax.broadcasted_iota(jnp.int32, (n_slot, rows), 1).astype(F32)
+    else:
+        count = mm(named.astype(BF16), before)
     picked = jnp.where(count == place, named, 0.0)
     comb = picked * share
     comb_hi = comb.astype(BF16)
@@ -285,7 +288,8 @@
     normed = (
         hf * lax.rsqrt(jnp.mean(hf * hf, axis=1, keepdims=True) + EPS) * nsc_ref[...]
     ).astype(BF16)
-    disp[...] = mm(picked.astype(BF16), normed, 0, 0).astype(BF16)
+    if not dense:
+        disp[...] = mm(picked.astype(BF16), normed).astype(BF16)
 
     def chunk(src, t):
         return al(src * n_tp + t)
@@ -295,17 +299,38 @@
         return pltpu.make_async_remote_copy(
             src_ref=disp.at[pl.ds(al(dest), capp)],
             dst_ref=xin.at[pl.ds(chunk(sp, tp), capp)],
-            send_sem=z_ss.at[o],
+            send_sem=z_ss.at[o, 0],
             recv_sem=ag_rs.at[sp, tp],
             device_id={"sp": dest},
         )
 
-    for o in range(1, n_sp):
-        z_copy(o).start()
-    xin[pl.ds(chunk(sp, tp), capp), :] = disp[pl.ds(al(sp), capp), :]
-
-    def source(i):
-        return (sp + i) % n_sp
+    def pass_on(src, up):
+        at = pl.ds(chunk(src, tp), capp)
+        return pltpu.make_async_remote_copy(
+            src_ref=xin.at[at],
+            dst_ref=xin.at[at],
+            send_sem=z_ss.at[src, 0 if up else 1],
+            recv_sem=ag_rs.at[src, tp],
+            device_id={"sp": (sp + 1) % n_sp if up else (sp + n_sp - 1) % n_sp},
+        )
+
+    def pass_along(src, act):
+        @pl.when((src <= sp) & (sp < n_sp - 1))
+        def _():
+            act(pass_on(src, True))
+
+        @pl.when((src >= sp) & (sp > 0))
+        def _():
+            act(pass_on(src, False))
+
+    if dense:
+        xin[pl.ds(chunk(sp, tp), capp), :] = normed
+        pass_along(sp, lambda c: c.start())
+    else:
+        for o in range(1, n_sp):
+            z_copy(o).start()
+        xin[pl.ds(chunk(sp, tp), capp), :] = disp[pl.ds(al(sp), capp), :]
+
 
     def tp_copy(src, t, sem, dest):
         return pltpu.make_async_remote_copy(
@@ -403,54 +428,60 @@
             acc = acc + fr_in[pl.ds(al(src * n_hi + o), capp), :].astype(F32)
         fin[pl.ds(al(src), capp), :] = acc.astype(BF16)
 
-    spread(0)
-    relay(0)
-    for w in weights[1:]:
-        w.wait()
-
     def z_arrived(i):
         src = source(i)
         pltpu.make_async_remote_copy(
-            src_ref=disp.at[pl.ds(0, capp)],
+            src_ref=xin.at[pl.ds(chunk(src, tp), capp)],
             dst_ref=xin.at[pl.ds(chunk(src, tp), capp)],
-            send_sem=z_ss.at[0],
+            send_sem=z_ss.at[0, 0],
             recv_sem=ag_rs.at[src, tp],
             device_id={"sp": (sp + 1) % n_sp},
         ).wait_recv()
-
+        if dense:
+            pass_along(src, lambda c: c.start())
+        spread(i)
+
+    spread(0)
+    relay(0)
     if n_sp > 1:
         z_arrived(1)
-        spread(1)
+    if n_sp > 2:
+
+        @pl.when(inner > 0)
+        def _():
+            z_arrived(2)
+
+    for w in weights[1:]:
+        w.wait()
 
     def body(i, carry):
         @pl.when(i < n_sp)
         def _():
             ffn(i)
 
+        @pl.when((i + 2 < n_sp) & ((i > 0) | (inner == 0)))
+        def _():
+            z_arrived(i + 2)
+
         @pl.when(i + 1 < n_sp)
         def _():
             relay(i + 1)
 
-        @pl.when(i + 2 < n_sp)
-        def _():
-            z_arrived(i + 2)
-            spread(i + 2)
-
-        @pl.when((i >= 1) & (i <= n_sp))
-        def _():
-            near_sum(i - 1)
+        @pl.when(i < n_sp)
+        def _():
+            near_sum(i)
+
+        @pl.when(i >= 1)
+        def _():
+            far_sum(i - 1)
 
         @pl.when(i >= 2)
         def _():
-            far_sum(i - 2)
-
-        @pl.when(i >= 3)
-        def _():
-            ret_copy(i - 2).start()
+            ret_copy(i - 1).start()
 
         return carry
 
-    lax.fori_loop(0, n_sp + 2, body, 0)
+    lax.fori_loop(0, n_sp + 1, body, 0)
 
     ret[pl.ds(al(sp), capp), :] = fin[pl.ds(al(sp), capp), :]
     for o in range(1, n_sp):
@@ -463,16 +494,19 @@
             device_id={"sp": src},
         ).wait_recv()
     back = ret[...]
-    out_ref[...] = (hid_s[...].astype(F32) + mm(comb_hi, back) + mm(comb_lo, back)).astype(BF16)
+    out_ref[...] = (hid_s[...].astype(F32) + mm(comb_hi, back, 0, 0) + mm(comb_lo, back, 0, 0)).astype(BF16)
 
     for o in range(1, n_sp):
         st_copy(o).wait_send()
-        z_copy(o).wait_send()
+        if not dense:
+            z_copy(o).wait_send()
         ret_copy(o).wait_send()
     for o in range(1, n_tp):
         rs_copy(o).wait_send()
 
     def drain(i, carry):
+        if dense:
+            pass_along(source(i), lambda c: c.wait_send())
         for h in range(1, n_hi):
             far_copy(i, h).wait_send()
             fr_copy(i, h).wait_send()
@@ -496,7 +530,8 @@
     de = args[15].shape[2]
     heads = args[11].shape[0]
     args = list(args)
-    args[10] = args[10].reshape(1, -1)
+    for i in (9, 13, 14):
+        args[i] = args[i].T
     args[12] = args[12].reshape(1, -1)
     vm = pl.BlockSpec(memory_space=pltpu.VMEM)
     hbm = pl.BlockSpec(memory_space=pl.ANY)
@@ -526,7 +561,7 @@
         dma((n_sp,)),
         dma((n_tp - 1,)),
         dma((n_tp - 1,)),
-        dma((n_sp,)),
+        dma((n_sp, 2)),
         dma((n_sp, n_hi)),
         dma((n_sp, n_hi)),
         dma((n_sp, n_tp)),

time: 72.5 us -> 63.4 us (0.87)
  local copies, waits for them, and re-layouts: 6.93 us -> 1.57 us
  Pallas kernels: 65.4 us -> 61.7 us
    unnamed x4 -> x1, local copies, waits for them, and re-layouts: 5.69 us -> 1.57 us
    pallas_call x1, Pallas kernels: 65.4 us -> 61.7 us  [local(): pl.pallas_call(functools.partial(kernel, n_sp, n_tp, cap, capp), out_shap...]
    reshape x1 -> x0, local copies, waits for them, and re-layouts: 1.24 us -> none  [local(): args[10] = args[10].reshape(1, -1)]
where the time goes in v2:
time: 63.4 us; the launch traced here: 63.3 us
  Pallas kernels  61.7 us (97%)
  local copies, waits for them, and re-layouts  1.57 us (2%)
    pallas_call x1, Pallas kernels, local(): pl.pallas_call(functools.partial(kernel, n_sp, n_tp, cap, capp), out_shap...  61.7 us
    unnamed x1, local copies, waits for them, and re-layouts  1.57 us

profile of v2, /device:TPU:0, one launch (start us, length us, event | category | flops | bytes accessed | tf_op | source)
XLA Modules:
  0.0 63.3 jit_solution(2046764183197788181)
XLA Ops:
  0.0 61.7 %shard_map.172 = bf16[32,2048]{1,0:T(8,128)(2,1)} custom-call(bf16[32,2048]{1,0:T(8,128)(2,1)} %skip_ref.1, bf16[128,128]{1,0:T(8,128)(2,1)} %wq_ref.1, bf16[128,128]{1,0:T(8,128)(2,1)} %nq_ref.1, bf16[128,128]{1,0:T(8,128)(2,1)} %wf_ref.1, bf16[128,128]{1,0:T(8,128)(2,1)} %nf_ref.1, f32[2,128]{1,0:T(2,128)} %wl_ref.1, f32[2,128]{1,0:T(2,128)} %nl_ref.1, ...), custom_call_target="tpu_custom_call" | custom-call | tf_op jit(solution)/shard_map/pallas_call | solution.py:575
  61.7 1.6 %copy.20 = bf16[32,2048]{1,0:T(8,128)(2,1)} copy(bf16[32,2048]{1,0:T(8,128)(2,1)} %shard_map.172) | data formatting | bytes 262144
